TPU v7x, 512 devices: a whole 4x4x16 slice. The times are simulated.
512 devices in a mesh: sp: 32 (over z, core), tp: 16 (over y, x).
Axes of the slice: x: 4, y: 4, z: 16, core: 2. Of those that a mesh axis runs over, the one named last changes fastest.
Arguments:
- residual: bfloat16 [6144, 2048], P('sp'), may hold values from -6 to 6
- query_in: bfloat16 [6144, 2048], P('sp', 'tp'), may hold values from -6 to 6
- value_in: bfloat16 [6144, 2048], P('sp', 'tp'), may hold values from -6 to 6
- forget_fwd: bfloat16 [6144, 2048], P('sp', 'tp'), may hold values from -4.5 to 4.5
- forget_bwd: bfloat16 [6144, 2048], P('sp', 'tp'), may hold values from -4.5 to 4.5
- jumps: float32 [16, 6144], P('tp', 'sp'), may hold values from -2.8 to 0
- gate_gap: float32 [2, 2048], P(None, 'tp'), may hold values from 0 to 0.1
- out_gate: bfloat16 [6144, 2048], P('sp', 'tp'), may hold values from -6 to 6
- head_gain: float32 [2048], P('tp'), may hold values from 0.1 to 1.9
- out_weight: bfloat16 [2048, 2048], P('tp'), may hold values from -0.25 to 0.25
- norm_gain: float32 [2048], replicated, may hold values from 0.1 to 1.9
- route_ids: int32 [6144, 4], P('sp'), may hold values from 0 to 31, all different within a row; in each aligned block of 192 rows (0 to 191, 192 to 383, ...) at most 36 rows name the same one
- route_weights: float32 [6144, 4], P('sp'), may hold values from 0.05 to 0.5
- w_gate: bfloat16 [32, 2048, 4096], P('sp', None, 'tp'), may hold values from -0.375 to 0.375
- w_up: bfloat16 [32, 2048, 4096], P('sp', None, 'tp'), may hold values from -0.375 to 0.375
- w_down: bfloat16 [32, 4096, 2048], P('sp', None, 'tp'), may hold values from -0.09375 to 0.09375
Outputs:
- mixed: bfloat16 [6144, 2048], P('sp', 'tp')
Inputs may be any that keep to these rules, and one draw needn't show every extreme that they name: `route_ids`: in each aligned block of 192 rows each expert is named by at most 36 rows, and by exactly 36 in some block; each row names 4 different experts.
All inputs are finite; a program needn't handle non-finite values.
Results may differ from a plain program's by a relative error of at most 0.024.
Values may be sent and summed in bfloat16 or wider, within the bound.
A program may use at most 64 MiB of HBM per device.

v0:
```python
import math
import jax
import jax.numpy as jnp
from jax import lax
from jax.sharding import Mesh
from jax.sharding import PartitionSpec as P

EXPERTS = 32
CAP = 36
SP = ("sp_0", "sp_1")
highest_precision = lax.Precision.HIGHEST
eps_norm = 1e-06
limit_value = 7.0
alpha_value = 1.702


def filled_with(x, identity):
    return jax.tree.map(
        lambda a, e: jnp.broadcast_to(jnp.asarray(e, a.dtype), a.shape), x, identity
    )


def all_in_one(x, axis):
    leaves = jax.tree.leaves(x)
    turns = sorted(range(len(leaves)), key=lambda k: -leaves[k].size)
    width = (1, *leaves[turns[0]].shape)[-1]
    lines = [
        jnp.pad(leaves[k].reshape(-1), (0, -leaves[k].size % width)).reshape(-1, width)
        for k in turns
    ]
    both, at, found = (lax.all_gather(jnp.concatenate(lines), axis), 0, {})
    for k, line in zip(turns, lines):
        section = both[:, at : at + len(line)].reshape(len(both), -1)
        found[k] = section[:, : leaves[k].size].reshape(-1, *leaves[k].shape)
        at += len(line)
    numbers = iter(range(len(leaves)))
    return jax.tree.map(lambda _: found[next(numbers)], x)


def entering(x, axes, combine, identity, reverse):
    before = start = filled_with(x, identity)
    running = x
    for axis in reversed(axes):
        length, index = (lax.axis_size(axis), lax.axis_index(axis))
        pieces = all_in_one(
            jax.tree.map(
                lambda part, kind: part.astype(kind),
                running,
                jax.tree.map(lambda a: jnp.bfloat16 if a.dtype == jnp.float32 else a.dtype, x),
            ),
            axis,
        )
        inside, running = (start, start)
        for k in reversed(range(length)) if reverse else range(length):
            passed = k > index if reverse else k < index
            running = combine(
                running, jax.tree.map(lambda part, own: part[k].astype(own.dtype), pieces, x)
            )
            inside = jax.tree.map(lambda new, old: jnp.where(passed, new, old), running, inside)
        before = combine(inside, before)
    return before


def in_blocks(x, dim, length):
    shape = x.shape
    pieces = x.reshape(*shape[:dim], length, shape[dim] // length, *shape[dim + 1 :])
    return jnp.moveaxis(pieces, dim, 0)


def sent_and_summed(x, axis, dim):
    length = lax.axis_size(axis)
    pieces = lax.all_to_all(in_blocks(x, dim, length), axis, 0, 0, tiled=True)
    return jnp.sum(pieces.astype(jnp.float32), axis=0)


def rows_for(lines, length):
    spare = -lines.shape[0] % length
    if not spare:
        return lines
    return jnp.concatenate([lines, jnp.zeros((spare, *lines.shape[1:]), lines.dtype)])


def in_order(pieces, dim):
    pieces = jnp.moveaxis(pieces, 0, dim)
    shape = pieces.shape
    return pieces.reshape(*shape[:dim], shape[dim] * shape[dim + 1], *shape[dim + 2 :])


def sent_to_all(x, axis):
    copies = jnp.broadcast_to(x, (lax.axis_size(axis), *x.shape))
    return lax.all_to_all(copies, axis, split_axis=0, concat_axis=0, tiled=True)


def gather_directly(x, axis, dim):
    return in_order(sent_to_all(x, axis), dim)


def sum_by_parts(x, axes):
    lines = x.reshape(-1, x.shape[-1])
    own = sent_and_summed(rows_for(lines, lax.axis_size(axes)), axes, 0)
    whole = gather_directly(own.astype(jnp.bfloat16), axes, 0)
    return whole[: len(lines)].reshape(x.shape).astype(jnp.float32)


def turned_blocks(pieces, axes, turns):
    inside = pieces.shape[1:]
    filled = pieces.reshape(*(lax.axis_size(a) for a in axes), *inside)
    for k in turns:
        filled = lax.all_to_all(filled, axes[k], k, k, tiled=True)
    return filled.reshape(-1, *inside)


def core_and_chips(x, groups, turns, split_dim, concat_dim):
    length = lax.axis_size(groups[0]) * lax.axis_size(groups[1])
    pieces = in_blocks(x, split_dim, length)
    return in_order(turned_blocks(pieces, groups, turns), concat_dim)


def block_pass(queries, keys_in, values, logs):
    head_rows, head_count, head_width = queries.shape
    block_size = math.gcd(head_rows, 64)
    block_count = head_rows // block_size

    def to_blocks(array):
        return array.reshape(block_count, block_size, head_count, array.shape[-1])

    q_block, k_block, v_block, log_block = (
        to_blocks(queries),
        to_blocks(keys_in),
        to_blocks(values),
        to_blocks(logs),
    )
    decay_sums = jnp.cumsum(log_block, axis=1)
    middle = decay_sums[:, block_size // 2 - 1 : block_size // 2]
    scores = jnp.einsum(
        "nthk,nshk->nhts",
        q_block * jnp.exp(decay_sums - middle),
        k_block * jnp.exp(middle - decay_sums),
        precision=highest_precision,
    )
    lower_mask = jnp.tril(jnp.ones((block_size, block_size), bool))
    within = jnp.einsum(
        "nhts,nshv->nthv", jnp.where(lower_mask, scores, 0.0), v_block, precision=highest_precision
    )
    block_end = decay_sums[:, -1]
    q_start = q_block * jnp.exp(decay_sums)
    k_end = k_block * jnp.exp(block_end[:, None] - decay_sums)

    def advance(current_state, block_items):
        query_segment, key_segment, value_segment, decay_part = block_items
        state_readout = jnp.einsum(
            "qwe,wei->qwi", query_segment, current_state, precision=highest_precision
        )
        current_state = current_state * jnp.exp(decay_part)[:, :, None] + jnp.einsum(
            "foj,fox->ojx", key_segment, value_segment, precision=highest_precision
        )
        return (current_state, state_readout)

    zero_state = jnp.zeros((head_count, head_width, values.shape[-1]), jnp.float32)
    final_state, across = lax.scan(advance, zero_state, (q_start, k_end, v_block, block_end))
    return ((within + across).reshape(head_rows, head_count, -1), final_state)


def combine_states(first_part, second_part):
    return (
        first_part[0] * second_part[0],
        second_part[0][:, :, None] * first_part[1] + second_part[1],
    )


def carried(queries, logs, running_state):
    decayed_state = queries * jnp.exp(jnp.cumsum(logs, axis=0))
    return jnp.einsum("una,nae->une", decayed_state, running_state, precision=highest_precision)


def shards(
    residual,
    query_in,
    value_in,
    forget_fwd,
    forget_bwd,
    jumps,
    gate_gap,
    out_gate,
    head_gain,
    out_weight,
    norm_gain,
    route_ids,
    route_weights,
    w_gate,
    w_up,
    w_down,
):
    head_rows, local_width = query_in.shape
    head_count = jumps.shape[0]
    head_width = local_width // head_count

    def by_head(array):
        return array.astype(jnp.float32).reshape(head_rows, head_count, head_width)

    queries = jax.nn.silu(by_head(query_in))
    values = by_head(value_in)
    jump_rows = jnp.transpose(jumps)[:, :, None]

    def gate_terms(forget_in, gap):
        key_share = gap.reshape(head_count, head_width) * jax.nn.sigmoid(-by_head(forget_in))
        return (key_share, jnp.log1p(-key_share) + jump_rows)

    keys_fwd, logs_fwd = gate_terms(forget_fwd, gate_gap[0])
    keys_bwd, logs_bwd = gate_terms(forget_bwd, gate_gap[1])
    ones_part = jnp.ones((head_count, head_width), jnp.float32)
    zero_part = jnp.zeros((head_count, head_width, head_width), jnp.float32)
    local_fwd, final_fwd = block_pass(queries, keys_fwd, values, logs_fwd)
    summary_fwd = (jnp.exp(jnp.sum(logs_fwd, axis=0)), final_fwd)
    carry_fwd = entering(summary_fwd, SP, combine_states, (ones_part, zero_part), False)[1]
    flip_queries = jnp.flip(queries, 0)
    flip_logs = jnp.flip(logs_bwd, 0)
    local_bwd, final_bwd = block_pass(
        flip_queries, jnp.flip(keys_bwd, 0), jnp.flip(values, 0), flip_logs
    )
    summary_bwd = (jnp.exp(jnp.sum(logs_bwd, axis=0)), final_bwd)
    carry_bwd = entering(summary_bwd, SP, combine_states, (ones_part, zero_part), True)[1]
    forward_out = local_fwd + carried(queries, logs_fwd, carry_fwd)
    backward_out = jnp.flip(local_bwd + carried(flip_queries, flip_logs, carry_bwd), 0)
    mixed_heads = forward_out + backward_out
    mean_square = jnp.mean(mixed_heads * mixed_heads, axis=-1, keepdims=True)
    normed = (mixed_heads * lax.rsqrt(mean_square + eps_norm)).reshape(head_rows, local_width)
    gated = (normed * head_gain * jax.nn.silu(out_gate.astype(jnp.float32))).astype(jnp.bfloat16)
    head_terms = jnp.dot(gated, out_weight, preferred_element_type=jnp.float32)
    summed = sum_by_parts(head_terms.astype(jnp.bfloat16), "tp")
    stream = (residual.astype(jnp.float32) + summed).astype(jnp.bfloat16)
    stream_f = stream.astype(jnp.float32)
    row_scale = lax.rsqrt(jnp.mean(stream_f * stream_f, axis=-1, keepdims=True) + eps_norm)
    normed_rows = (stream_f * row_scale * norm_gain).astype(jnp.bfloat16)
    top_count = route_ids.shape[1]
    flat_ids = route_ids.reshape(-1)
    one_hot = (flat_ids[:, None] == jnp.arange(EXPERTS, dtype=jnp.int32)[None, :]).astype(jnp.int32)
    slot_rank = jnp.sum((jnp.cumsum(one_hot, axis=0) - 1) * one_hot, axis=1)
    slot_index = flat_ids * CAP + slot_rank
    owner_rows = jnp.arange(head_rows * top_count, dtype=jnp.int32) // top_count
    slot_rows = jnp.full((EXPERTS * CAP,), head_rows, jnp.int32).at[slot_index].set(owner_rows)
    padded_rows = jnp.concatenate(
        [normed_rows, jnp.zeros((1, normed_rows.shape[1]), jnp.bfloat16)], axis=0
    )
    tp_index = lax.axis_index("tp")
    part_width = w_down.shape[2]
    column_rows = lax.dynamic_slice_in_dim(padded_rows, tp_index * part_width, part_width, 1)
    buffer = column_rows[slot_rows].reshape(EXPERTS, CAP, part_width)
    arrived = lax.all_to_all(buffer, SP, split_axis=0, concat_axis=1, tiled=True)
    piece = lax.all_gather(arrived, "tp", axis=2, tiled=True)
    gate_sum = jnp.einsum("esd,edf->esf", piece, w_gate, preferred_element_type=jnp.float32)
    up_sum = jnp.einsum("esd,edf->esf", piece, w_up, preferred_element_type=jnp.float32)
    gate_sum = jnp.minimum(gate_sum, limit_value)
    up_sum = jnp.clip(up_sum, -limit_value, limit_value)
    active = (gate_sum * jax.nn.sigmoid(alpha_value * gate_sum) * (up_sum + 1.0)).astype(
        jnp.bfloat16
    )
    produced = jnp.einsum(
        "esf,efd->esd",
        lax.all_gather(active, "tp", axis=2, tiled=True),
        w_down,
        preferred_element_type=jnp.float32,
    ).astype(jnp.bfloat16)
    returned = core_and_chips(produced, ("sp_0", "sp_1"), (1, 0), 1, 0)
    picked = returned.reshape(EXPERTS * CAP, part_width)[slot_index].astype(jnp.float32)
    picked = picked.reshape(head_rows, top_count, part_width)
    moe_out = jnp.sum(picked * route_weights[:, :, None], axis=1)
    own_columns = lax.dynamic_slice_in_dim(stream_f, tp_index * part_width, part_width, 1)
    return (own_columns + moe_out).astype(jnp.bfloat16)


def solution(mesh):
    finer = Mesh(mesh.devices.reshape(16, 2, mesh.shape["tp"]), ("sp_0", "sp_1", "tp"))
    return jax.shard_map(
        shards,
        mesh=finer,
        in_specs=(
            P(SP, None),
            P(SP, "tp"),
            P(SP, "tp"),
            P(SP, "tp"),
            P(SP, "tp"),
            P("tp", SP),
            P(None, "tp"),
            P(SP, "tp"),
            P("tp"),
            P("tp", None),
            P(),
            P(SP, None),
            P(SP, None),
            P(SP, None, "tp"),
            P(SP, None, "tp"),
            P(SP, None, "tp"),
        ),
        out_specs=P(SP, "tp"),
        check_vma=False,
    )
```

profile of v0, /device:TPU:2, one launch (start us, length us, event | category | flops | bytes accessed | tf_op | source)
XLA Modules:
  0.0 397.6 jit_solution(2136767596949991621)
XLA Ops:
  7.3 1.0 fusion.388
  10.9 1.7 while.26
  12.6 1.9 all-gather.5
  15.2 38.4 %all-gather.6 = bf16[16,129,128]{2,1,0:T(8,128)(2,1)S(1)} all-gather(bf16[1,129,128]{2,1,0:T(8,128)(2,1)S(1)} %maximum_bitcast_fusion.1), channel_id=3, replica_groups=mesh['sp_0'=16,'sp_1'=2,'tp'=16] {'sp_0'}, dimensions={0}, use_global_device_ids=true | all-gather | bytes 561408 | tf_op jit(solution)/shard_map/all_gather | solution.py:31
  56.6 1.7 while.27
  58.4 1.9 all-gather.7
  61.0 29.2 %all-gather.8 = bf16[16,129,128]{2,1,0:T(8,128)(2,1)S(1)} all-gather(bf16[1,129,128]{2,1,0:T(8,128)(2,1)S(1)} %maximum_bitcast_fusion.3), channel_id=5, replica_groups=mesh['sp_0'=16,'sp_1'=2,'tp'=16] {'sp_0'}, dimensions={0}, use_global_device_ids=true | all-gather | bytes 561408 | tf_op jit(solution)/shard_map/all_gather | solution.py:31
  92.2 1.1 fusion.41
  93.5 1.5 fusion.39
  96.0 1.6 multiply_reduce_fusion.1
  98.1 1.2 reshape.1657
  99.3 7.5 %all-to-all-start = ((bf16[16,12,2048]{2,1,0:T(8,128)(2,1)}), bf16[16,12,2048]{2,1,0:T(8,128)(2,1)S(1)}, u32[]{:S(2)}, u32[]{:S(2)}) async-start(bf16[16,12,2048]{2,1,0:T(8,128)(2,1)} %reshape.1657), calls=%async_computation | async-start | bytes 2097152 | tf_op jit(solution)/shard_map/all_to_all | solution.py:72
  107.0 1.7 reduce-window.26
  108.7 9.9 %all-to-all-done = bf16[16,12,2048]{2,1,0:T(8,128)(2,1)S(1)} async-done(((bf16[16,12,2048]{2,1,0:T(8,128)(2,1)}), bf16[16,12,2048]{2,1,0:T(8,128)(2,1)S(1)}, u32[]{:S(2)}, u32[]{:S(2)}) %all-to-all-start) | async-done | bytes 786464 | tf_op jit(solution)/shard_map/all_to_all | solution.py:72
  118.8 1.1 broadcast_in_dim.35
  120.0 5.0 %all-to-all-start.1 = ((bf16[16,12,2048]{2,1,0:T(8,128)(2,1)}), bf16[16,12,2048]{2,1,0:T(8,128)(2,1)S(1)}, u32[]{:S(2)}, u32[]{:S(2)}) async-start(bf16[16,12,2048]{2,1,0:T(8,128)(2,1)} %broadcast_in_dim.35), calls=%async_computation.1 | async-start | bytes 2097152 | tf_op jit(solution)/shard_map/all_to_all | solution.py:91
  125.7 3.4 scatter_custom_fusion
  129.2 7.8 %all-to-all-done.1 = bf16[16,12,2048]{2,1,0:T(8,128)(2,1)S(1)} async-done(((bf16[16,12,2048]{2,1,0:T(8,128)(2,1)}), bf16[16,12,2048]{2,1,0:T(8,128)(2,1)S(1)}, u32[]{:S(2)}, u32[]{:S(2)}) %all-to-all-start.1) | async-done | bytes 786464 | tf_op jit(solution)/shard_map/all_to_all | solution.py:91
  136.9 1.3 reshape.1699
  138.3 1.7 multiply_reduce_fusion
  140.2 2.9 gather_fusion
  143.2 33.2 %all_to_all.32 = bf16[32,36,128]{2,1,0:T(8,128)(2,1)S(1)} all-to-all(bf16[32,36,128]{2,1,0:T(8,128)(2,1)S(1)} %reshape.1659), channel_id=1, replica_groups=mesh['sp_0'=16,'sp_1'=2,'tp'=16] {'sp_0','sp_1'}, dimensions={0} | all-to-all | bytes 589824 | tf_op jit(solution)/shard_map/all_to_all | solution.py:249
  177.5 62.6 %all-gather.12.cloned.1.call-done = bf16[1,1152,2048]{2,1,0:T(8,128)(2,1)} async-done(((bf16[1,1152,128]{2,1,0:T(8,128)(2,1)}), bf16[1,1152,2048]{2,1,0:T(8,128)(2,1)}) %all-gather.12.cloned.1.call-update) | async-done | bytes 4718608 | tf_op jit(solution)/shard_map/all_gather | solution.py:250
  240.1 3.9 fusion.25
  244.1 2.4 fusion.34
  246.6 97.4 %all-gather.14.cloned.1.call-done = bf16[1152,4096]{1,0:T(8,128)(2,1)} async-done(((bf16[1152,256]{1,0:T(8,128)(2,1)}), bf16[1152,4096]{1,0:T(8,128)(2,1)}) %all-gather.14.cloned.1.call-update) | async-done | bytes 9437200 | tf_op jit(solution)/shard_map/all_gather | solution.py:260
  344.0 6.5 %convolution_convert_fusion.1 = bf16[1152,128]{1,0:T(8,128)(2,1)S(1)} fusion(bf16[1152,4096]{1,0:T(8,128)(2,1)} %all-gather.14.cloned.1.call-done, bf16[1,4096,128]{2,1,0:T(8,128)(2,1)} %param.35), kind=kOutput, calls=%fused_computation.43 | convolution fusion | flops 1208107008 | bytes 10780672 | tf_op jit(solution)/shard_map/esf,efd->esd/dot_general | solution.py:258
  350.7 4.0 all_to_all.33
  354.6 1.0 copy.64
  355.6 12.3 %all-to-all-start.4 = ((bf16[16,2,1,36,128]{4,1,3,2,0:T(2,128)(2,1)}), bf16[16,2,1,36,128]{4,1,3,2,0:T(2,128)(2,1)S(1)}, u32[]{:S(2)}, u32[]{:S(2)}) async-start(bf16[16,2,1,36,128]{4,1,3,2,0:T(2,128)(2,1)} %copy.64), calls=%async_computation.4 | async-start | bytes 589824 | tf_op jit(solution)/shard_map/all_to_all | solution.py:109
  368.1 19.8 %all-to-all-done.4 = bf16[16,2,1,36,128]{4,1,3,2,0:T(2,128)(2,1)S(1)} async-done(((bf16[16,2,1,36,128]{4,1,3,2,0:T(2,128)(2,1)}), bf16[16,2,1,36,128]{4,1,3,2,0:T(2,128)(2,1)S(1)}, u32[]{:S(2)}, u32[]{:S(2)}) %all-to-all-start.4) | async-done | bytes 294944 | tf_op jit(solution)/shard_map/all_to_all | solution.py:109
  387.9 1.9 gather_fusion.1
  (204 shorter events, 17.9 us)
Async XLA Ops:
  6.5 233.5 %copy-start = (bf16[1,2048,256]{2,1,0:T(8,128)(2,1)S(1)}, bf16[1,2048,256]{2,1,0:T(8,128)(2,1)}, u32[]{:S(2)}) copy-start(bf16[1,2048,256]{2,1,0:T(8,128)(2,1)} %param.33) | copy-start | bytes 3145732
  10.9 44.1 %copy-start.3 = (bf16[192,128]{1,0:T(8,128)(2,1)S(1)}, bf16[192,128]{1,0:T(8,128)(2,1)}, u32[]{:S(2)}) copy-start(bf16[192,128]{1,0:T(8,128)(2,1)} %param.22) | copy-start | bytes 147460
  12.6 41.7 %copy-start.4 = (f32[3,64,1,128]{3,1,2,0:T(8,128)}, f32[3,64,1,128]{3,1,2,0:T(8,128)S(1)}, u32[]{:S(2)}) copy-start(f32[3,64,1,128]{3,1,2,0:T(8,128)S(1)} %get-tuple-element.81) | copy-start | bytes 294916
  14.5 40.9 %copy-start.7 = (bf16[2,129,128]{2,1,0:T(8,128)(2,1)}, bf16[2,129,128]{2,1,0:T(8,128)(2,1)S(1)}, u32[]{:S(2)}) copy-start(bf16[2,129,128]{2,1,0:T(8,128)(2,1)S(1)} %all-gather.5) | copy-start | bytes 198148
  14.5 40.9 %copy-start.19 = (f32[128]{0:T(128)}, f32[128]{0:T(128)S(1)}, u32[]{:S(2)}) copy-start(f32[128]{0:T(128)S(1)} %fusion.382) | copy-start | bytes 1540
  15.1 40.3 %copy-start.16 = (f32[128]{0:T(128)}, f32[128]{0:T(128)S(1)}, u32[]{:S(2)}) copy-start(f32[128]{0:T(128)S(1)} %get-tuple-element.212) | copy-start | bytes 1540
  58.3 2.6 copy-start.6
  58.3 33.5 %copy-start.12 = (f32[3,128]{1,0:T(4,128)S(1)}, f32[3,128]{1,0:T(4,128)}, u32[]{:S(2)}) copy-start(f32[3,128]{1,0:T(4,128)} %get-tuple-element.225) | copy-start | bytes 4612
  60.2 31.1 %copy-start.8 = (bf16[2,129,128]{2,1,0:T(8,128)(2,1)}, bf16[2,129,128]{2,1,0:T(8,128)(2,1)S(1)}, u32[]{:S(2)}) copy-start(bf16[2,129,128]{2,1,0:T(8,128)(2,1)S(1)} %all-gather.7) | copy-start | bytes 198148
  92.1 3.2 copy-start.11
  93.3 2.6 copy-start.10
  93.3 2.6 copy-start.17
  93.3 2.6 copy-start.20
  93.3 2.6 copy-start.21
  93.3 2.6 copy-start.22
  93.3 2.6 copy-start.23
  93.4 2.6 copy-start.24
  93.4 2.6 copy-start.25
  93.4 2.6 copy-start.26
  93.4 2.6 copy-start.27
  93.4 2.6 copy-start.28
  93.4 2.6 copy-start.29
  98.1 8.7 %copy-start.13 = (s32[192,4]{0,1:T(4,128)S(1)}, s32[192,4]{0,1:T(4,128)}, u32[]{:S(2)}) copy-start(s32[192,4]{0,1:T(4,128)} %param.31) | copy-start | bytes 9220
  99.3 19.4 %all-to-all-start = ((bf16[16,12,2048]{2,1,0:T(8,128)(2,1)}), bf16[16,12,2048]{2,1,0:T(8,128)(2,1)S(1)}, u32[]{:S(2)}, u32[]{:S(2)}) async-start(bf16[16,12,2048]{2,1,0:T(8,128)(2,1)} %reshape.1657), calls=%async_computation | async-start | bytes 2097152 | tf_op jit(solution)/shard_map/all_to_all | solution.py:72
  120.0 17.0 %all-to-all-start.1 = ((bf16[16,12,2048]{2,1,0:T(8,128)(2,1)}), bf16[16,12,2048]{2,1,0:T(8,128)(2,1)S(1)}, u32[]{:S(2)}, u32[]{:S(2)}) async-start(bf16[16,12,2048]{2,1,0:T(8,128)(2,1)} %broadcast_in_dim.35), calls=%async_computation.1 | async-start | bytes 2097152 | tf_op jit(solution)/shard_map/all_to_all | solution.py:91
  124.9 115.1 %all-gather.12.cloned.1.call-start = ((), (), s32[]{:S(2)}) async-start(), calls=%async_computation.5 | async-start | bytes 5013504 | tf_op jit(solution)/shard_map/all_gather | solution.py:250
  125.2 13.1 %copy-start.1 = (bf16[192,2048]{1,0:T(8,128)(2,1)S(1)}, bf16[192,2048]{1,0:T(8,128)(2,1)}, u32[]{:S(2)}) copy-start(bf16[192,2048]{1,0:T(8,128)(2,1)} %param.20) | copy-start | bytes 2359300
  177.3 166.7 %all-gather.14.cloned.1.call-start = ((), (), s32[]{:S(2)}) async-start(), calls=%async_computation.6 | async-start | bytes 10027008 | tf_op jit(solution)/shard_map/all_gather | solution.py:260
  240.1 3.9 copy-start.37
  240.1 4.1 %copy-start.38 = (bf16[1,2048,256]{2,1,0:T(8,128)(2,1)S(1)}, bf16[1,2048,256]{2,1,0:T(8,128)(2,1)}, u32[]{:S(2)}) copy-start(bf16[1,2048,256]{2,1,0:T(8,128)(2,1)} %param.34) | copy-start | bytes 3145732
  350.5 17.4 %copy-start.15 = (f32[192,4]{0,1:T(4,128)S(1)}, f32[192,4]{0,1:T(4,128)}, u32[]{:S(2)}) copy-start(f32[192,4]{0,1:T(4,128)} %param.32) | copy-start | bytes 9220
  355.6 32.2 %all-to-all-start.4 = ((bf16[16,2,1,36,128]{4,1,3,2,0:T(2,128)(2,1)}), bf16[16,2,1,36,128]{4,1,3,2,0:T(2,128)(2,1)S(1)}, u32[]{:S(2)}, u32[]{:S(2)}) async-start(bf16[16,2,1,36,128]{4,1,3,2,0:T(2,128)(2,1)} %copy.64), calls=%async_computation.4 | async-start | bytes 589824 | tf_op jit(solution)/shard_map/all_to_all | solution.py:109
  (13 other events, 31.5 us)
Sparse Core Ops, SparseCore 0:
  177.4 62.6 all-gather.11
  246.7 97.2 all-gather.13
where the time goes:
time: 398 us
  waiting for transfers between devices  197 us (49%)
  blocking collectives  108 us (27%)
  starting transfers between devices  25 us (6%)
  matrix products  21.1 us (5%)
  local copies, waits for them, and re-layouts  18.4 us (5%)
  between operations  14.5 us (4%)
  other arithmetic  12.4 us (3%)
    all_gather x1, waiting for transfers between devices, shards(): lax.all_gather(active, 'tp', axis=2, tiled=True)  97.4 us
    all_gather x4, blocking collectives, all_in_one(): both, at, found = (lax.all_gather(jnp.concatenate(lines), axis), 0, {})  71.3 us
    all_gather x1, waiting for transfers between devices, shards(): piece = lax.all_gather(arrived, 'tp', axis=2, tiled=True)  62.6 us
    all_to_all x1, blocking collectives, shards(): lax.all_to_all(buffer, SP, split_axis=0, concat_axis=1, tiled=True)  33.2 us
    all_to_all x1, waiting for transfers between devices, turned_blocks(): filled = lax.all_to_all(filled, axes[k], k, k, tiled=True)  19.8 us
    all_to_all x1, starting transfers between devices, turned_blocks(): filled = lax.all_to_all(filled, axes[k], k, k, tiled=True)  12.3 us
    all_to_all x1, waiting for transfers between devices, sent_and_summed(): pieces = lax.all_to_all(in_blocks(x, dim, length), axis, 0, 0, tiled=True)  9.91 us
  transfers between devices with their start and end apart: 5, of which 5 were waited for; matrix products, arithmetic and copies ran while one was open for 2% of the time, Pallas kernels for 0%

commit v1 on v0

--- a/solution.py
+++ b/solution.py
@@ -247,7 +247,8 @@
     column_rows = lax.dynamic_slice_in_dim(padded_rows, tp_index * part_width, part_width, 1)
     buffer = column_rows[slot_rows].reshape(EXPERTS, CAP, part_width)
     arrived = lax.all_to_all(buffer, SP, split_axis=0, concat_axis=1, tiled=True)
-    piece = lax.all_gather(arrived, "tp", axis=2, tiled=True)
+    sent = jnp.stack([arrived] * lax.axis_size("tp"))
+    piece = jnp.concatenate(lax.all_to_all(sent, "tp", 0, 0), axis=2)
     gate_sum = jnp.einsum("esd,edf->esf", piece, w_gate, preferred_element_type=jnp.float32)
     up_sum = jnp.einsum("esd,edf->esf", piece, w_up, preferred_element_type=jnp.float32)
     gate_sum = jnp.minimum(gate_sum, limit_value)

time: 398 us -> 386 us (0.970)
  waiting for transfers between devices: 197 us -> 126 us
  blocking collectives: 108 us -> 168 us
    all_gather x1 -> x0, waiting for transfers between devices: 62.6 us -> none  [shards(): piece = lax.all_gather(arrived, 'tp', axis=2, tiled=True)]
    all_to_all x0 -> x1, blocking collectives: none -> 59.4 us  [shards(): piece = jnp.concatenate(lax.all_to_all(sent, 'tp', 0, 0), axis=2)]
    all_gather x1, waiting for transfers between devices: 97.4 us -> 88.5 us  [shards(): lax.all_gather(active, 'tp', axis=2, tiled=True)]
  transfers between devices with their start and end apart: 5 -> 4, of which waited for: 5 -> 4; matrix products, arithmetic and copies ran while one was open for 2% -> 2% of each run, Pallas kernels for 0% -> 0%
where the time goes in v1:
time: 386 us; the launch traced here: 385 us
  blocking collectives  168 us (44%)
  waiting for transfers between devices  126 us (33%)
  starting transfers between devices  24.8 us (6%)
  local copies, waits for them, and re-layouts  20.1 us (5%)
  matrix products  18.5 us (5%)
  between operations  14.7 us (4%)
  other arithmetic  12.5 us (3%)
    all_gather x1, waiting for transfers between devices, shards(): lax.all_gather(active, 'tp', axis=2, tiled=True)  88.5 us
    all_gather x4, blocking collectives, all_in_one(): both, at, found = (lax.all_gather(jnp.concatenate(lines), axis), 0, {})  71.3 us
    all_to_all x1, blocking collectives, shards(): piece = jnp.concatenate(lax.all_to_all(sent, 'tp', 0, 0), axis=2)  59.4 us
    all_to_all x1, blocking collectives, shards(): lax.all_to_all(buffer, SP, split_axis=0, concat_axis=1, tiled=True)  33.2 us
    all_to_all x1, waiting for transfers between devices, turned_blocks(): filled = lax.all_to_all(filled, axes[k], k, k, tiled=True)  19.8 us
    all_to_all x1, starting transfers between devices, turned_blocks(): filled = lax.all_to_all(filled, axes[k], k, k, tiled=True)  12.3 us
    all_to_all x1, waiting for transfers between devices, sent_and_summed(): pieces = lax.all_to_all(in_blocks(x, dim, length), axis, 0, 0, tiled=True)  9.91 us
    all_to_all x1, waiting for transfers between devices, sent_to_all(): return lax.all_to_all(copies, axis, split_axis=0, concat_axis=0, tiled=True)  7.78 us
  transfers between devices with their start and end apart: 4, of which 4 were waited for; matrix products, arithmetic and copies ran while one was open for 2% of the time, Pallas kernels for 0%

profile of v1, /device:TPU:2, one launch (start us, length us, event | category | flops | bytes accessed | tf_op | source)
XLA Modules:
  0.0 384.8 jit_solution(6561677924764157860)
XLA Ops:
  10.9 1.7 while.26
  12.7 1.9 all-gather.5
  15.2 38.4 %all-gather.6 = bf16[16,129,128]{2,1,0:T(8,128)(2,1)S(1)} all-gather(bf16[1,129,128]{2,1,0:T(8,128)(2,1)S(1)} %maximum_bitcast_fusion.1), channel_id=3, replica_groups=mesh['sp_0'=16,'sp_1'=2,'tp'=16] {'sp_0'}, dimensions={0}, use_global_device_ids=true | all-gather | bytes 561408 | tf_op jit(solution)/shard_map/all_gather | solution.py:31
  56.5 1.7 while.27
  58.3 1.9 all-gather.7
  60.9 29.2 %all-gather.8 = bf16[16,129,128]{2,1,0:T(8,128)(2,1)S(1)} all-gather(bf16[1,129,128]{2,1,0:T(8,128)(2,1)S(1)} %maximum_bitcast_fusion.3), channel_id=5, replica_groups=mesh['sp_0'=16,'sp_1'=2,'tp'=16] {'sp_0'}, dimensions={0}, use_global_device_ids=true | all-gather | bytes 561408 | tf_op jit(solution)/shard_map/all_gather | solution.py:31
  92.2 1.1 fusion.25
  93.6 1.5 fusion.23
  96.1 1.6 multiply_reduce_fusion.1
  98.2 1.2 reshape.1668
  99.4 7.5 %all-to-all-start = ((bf16[16,12,2048]{2,1,0:T(8,128)(2,1)}), bf16[16,12,2048]{2,1,0:T(8,128)(2,1)S(1)}, u32[]{:S(2)}, u32[]{:S(2)}) async-start(bf16[16,12,2048]{2,1,0:T(8,128)(2,1)} %reshape.1668), calls=%async_computation | async-start | bytes 2097152 | tf_op jit(solution)/shard_map/all_to_all | solution.py:72
  107.1 1.7 reduce-window.26
  108.8 9.9 %all-to-all-done = bf16[16,12,2048]{2,1,0:T(8,128)(2,1)S(1)} async-done(((bf16[16,12,2048]{2,1,0:T(8,128)(2,1)}), bf16[16,12,2048]{2,1,0:T(8,128)(2,1)S(1)}, u32[]{:S(2)}, u32[]{:S(2)}) %all-to-all-start) | async-done | bytes 786464 | tf_op jit(solution)/shard_map/all_to_all | solution.py:72
  119.0 1.1 broadcast_in_dim.35
  120.1 5.0 %all-to-all-start.1 = ((bf16[16,12,2048]{2,1,0:T(8,128)(2,1)}), bf16[16,12,2048]{2,1,0:T(8,128)(2,1)S(1)}, u32[]{:S(2)}, u32[]{:S(2)}) async-start(bf16[16,12,2048]{2,1,0:T(8,128)(2,1)} %broadcast_in_dim.35), calls=%async_computation.1 | async-start | bytes 2097152 | tf_op jit(solution)/shard_map/all_to_all | solution.py:91
  125.8 3.4 scatter_custom_fusion
  129.3 7.8 %all-to-all-done.1 = bf16[16,12,2048]{2,1,0:T(8,128)(2,1)S(1)} async-done(((bf16[16,12,2048]{2,1,0:T(8,128)(2,1)}), bf16[16,12,2048]{2,1,0:T(8,128)(2,1)S(1)}, u32[]{:S(2)}, u32[]{:S(2)}) %all-to-all-start.1) | async-done | bytes 786464 | tf_op jit(solution)/shard_map/all_to_all | solution.py:91
  137.0 1.3 reshape.1711
  138.4 1.9 multiply_reduce_fusion
  140.5 2.9 gather_fusion
  143.5 33.2 %all_to_all.34 = bf16[32,36,128]{2,1,0:T(8,128)(2,1)S(1)} all-to-all(bf16[32,36,128]{2,1,0:T(8,128)(2,1)S(1)} %reshape.1670), channel_id=1, replica_groups=mesh['sp_0'=16,'sp_1'=2,'tp'=16] {'sp_0','sp_1'}, dimensions={0} | all-to-all | bytes 589824 | tf_op jit(solution)/shard_map/all_to_all | solution.py:249
  177.5 1.2 copy.64
  179.3 59.4 %all_to_all.35 = bf16[16,1,1152,128]{2,3,1,0:T(8,128)(2,1)S(1)} all-to-all(bf16[16,1,1152,128]{2,3,1,0:T(8,128)(2,1)S(1)} %stack.5), channel_id=1, replica_groups=mesh['sp_0'=16,'sp_1'=2,'tp'=16] {'tp'}, dimensions={0} | all-to-all | bytes 9437184 | tf_op jit(solution)/shard_map/all_to_all | solution.py:251
  238.7 1.4 convolution_minimum_fusion
  240.2 2.4 fusion.20
  242.6 88.5 %all-gather.11.cloned.1.call-done = bf16[1152,4096]{1,0:T(8,128)(2,1)} async-done(((bf16[1152,256]{1,0:T(8,128)(2,1)}), bf16[1152,4096]{1,0:T(8,128)(2,1)}) %all-gather.11.cloned.1.call-update) | async-done | bytes 9437200 | tf_op jit(solution)/shard_map/all_gather | solution.py:261
  331.2 6.5 %convolution_convert_fusion.1 = bf16[1152,128]{1,0:T(8,128)(2,1)S(1)} fusion(bf16[1152,4096]{1,0:T(8,128)(2,1)} %all-gather.11.cloned.1.call-done, bf16[1,4096,128]{2,1,0:T(8,128)(2,1)} %param.35), kind=kOutput, calls=%fused_computation.39 | convolution fusion | flops 1208107008 | bytes 10780672 | tf_op jit(solution)/shard_map/esf,efd->esd/dot_general | solution.py:259
  337.8 4.0 %all_to_all.36 = bf16[16,2,1,36,128]{4,0,3,2,1:T(8,128)(2,1)S(1)} all-to-all(bf16[16,2,1,36,128]{4,0,3,2,1:T(8,128)(2,1)S(1)} %copy.66), channel_id=1, replica_groups=mesh['sp_0'=16,'sp_1'=2,'tp'=16] {'sp_1'}, dimensions={1} | all-to-all | bytes 589824 | tf_op jit(solution)/shard_map/all_to_all | solution.py:109
  341.8 1.0 copy.67
  342.8 12.3 %all-to-all-start.5 = ((bf16[16,2,1,36,128]{4,1,3,2,0:T(2,128)(2,1)}), bf16[16,2,1,36,128]{4,1,3,2,0:T(2,128)(2,1)S(1)}, u32[]{:S(2)}, u32[]{:S(2)}) async-start(bf16[16,2,1,36,128]{4,1,3,2,0:T(2,128)(2,1)} %copy.67), calls=%async_computation.5 | async-start | bytes 589824 | tf_op jit(solution)/shard_map/all_to_all | solution.py:109
  355.2 19.8 %all-to-all-done.5 = bf16[16,2,1,36,128]{4,1,3,2,0:T(2,128)(2,1)S(1)} async-done(((bf16[16,2,1,36,128]{4,1,3,2,0:T(2,128)(2,1)}), bf16[16,2,1,36,128]{4,1,3,2,0:T(2,128)(2,1)S(1)}, u32[]{:S(2)}, u32[]{:S(2)}) %all-to-all-start.5) | async-done | bytes 294944 | tf_op jit(solution)/shard_map/all_to_all | solution.py:109
  375.1 1.9 gather_fusion.1
  (218 shorter events, 19.1 us)
Async XLA Ops:
  6.5 232.2 %copy-start = (bf16[1,2048,256]{2,1,0:T(8,128)(2,1)S(1)}, bf16[1,2048,256]{2,1,0:T(8,128)(2,1)}, u32[]{:S(2)}) copy-start(bf16[1,2048,256]{2,1,0:T(8,128)(2,1)} %param.33) | copy-start | bytes 3145732
  10.9 44.0 %copy-start.2 = (bf16[192,128]{1,0:T(8,128)(2,1)S(1)}, bf16[192,128]{1,0:T(8,128)(2,1)}, u32[]{:S(2)}) copy-start(bf16[192,128]{1,0:T(8,128)(2,1)} %param.22) | copy-start | bytes 147460
  12.6 42.2 %copy-start.3 = (f32[3,64,1,128]{3,1,2,0:T(8,128)}, f32[3,64,1,128]{3,1,2,0:T(8,128)S(1)}, u32[]{:S(2)}) copy-start(f32[3,64,1,128]{3,1,2,0:T(8,128)S(1)} %get-tuple-element.81) | copy-start | bytes 294916
  14.5 40.6 %copy-start.6 = (bf16[2,129,128]{2,1,0:T(8,128)(2,1)}, bf16[2,129,128]{2,1,0:T(8,128)(2,1)S(1)}, u32[]{:S(2)}) copy-start(bf16[2,129,128]{2,1,0:T(8,128)(2,1)S(1)} %all-gather.5) | copy-start | bytes 198148
  14.5 40.6 %copy-start.18 = (f32[128]{0:T(128)}, f32[128]{0:T(128)S(1)}, u32[]{:S(2)}) copy-start(f32[128]{0:T(128)S(1)} %fusion.366) | copy-start | bytes 1540
  15.1 40.0 %copy-start.15 = (f32[128]{0:T(128)}, f32[128]{0:T(128)S(1)}, u32[]{:S(2)}) copy-start(f32[128]{0:T(128)S(1)} %get-tuple-element.212) | copy-start | bytes 1540
  58.2 2.6 copy-start.5
  58.2 33.6 %copy-start.11 = (f32[3,128]{1,0:T(4,128)S(1)}, f32[3,128]{1,0:T(4,128)}, u32[]{:S(2)}) copy-start(f32[3,128]{1,0:T(4,128)} %get-tuple-element.225) | copy-start | bytes 4612
  60.1 31.1 %copy-start.7 = (bf16[2,129,128]{2,1,0:T(8,128)(2,1)}, bf16[2,129,128]{2,1,0:T(8,128)(2,1)S(1)}, u32[]{:S(2)}) copy-start(bf16[2,129,128]{2,1,0:T(8,128)(2,1)S(1)} %all-gather.7) | copy-start | bytes 198148
  92.2 3.2 copy-start.10
  93.4 2.5 copy-start.9
  93.4 2.5 copy-start.16
  93.4 2.5 copy-start.19
  93.5 2.5 copy-start.20
  93.5 2.5 copy-start.21
  93.5 2.5 copy-start.22
  93.5 2.5 copy-start.23
  93.5 2.5 copy-start.24
  93.5 2.5 copy-start.25
  93.5 2.5 copy-start.26
  93.5 2.5 copy-start.27
  93.5 2.5 copy-start.28
  93.5 2.5 copy-start.29
  93.6 2.5 copy-start.30
  93.6 2.5 copy-start.31
  93.6 2.5 copy-start.32
  98.2 8.7 %copy-start.12 = (s32[192,4]{0,1:T(4,128)S(1)}, s32[192,4]{0,1:T(4,128)}, u32[]{:S(2)}) copy-start(s32[192,4]{0,1:T(4,128)} %param.31) | copy-start | bytes 9220
  99.4 19.4 %all-to-all-start = ((bf16[16,12,2048]{2,1,0:T(8,128)(2,1)}), bf16[16,12,2048]{2,1,0:T(8,128)(2,1)S(1)}, u32[]{:S(2)}, u32[]{:S(2)}) async-start(bf16[16,12,2048]{2,1,0:T(8,128)(2,1)} %reshape.1668), calls=%async_computation | async-start | bytes 2097152 | tf_op jit(solution)/shard_map/all_to_all | solution.py:72
  120.1 17.0 %all-to-all-start.1 = ((bf16[16,12,2048]{2,1,0:T(8,128)(2,1)}), bf16[16,12,2048]{2,1,0:T(8,128)(2,1)S(1)}, u32[]{:S(2)}, u32[]{:S(2)}) async-start(bf16[16,12,2048]{2,1,0:T(8,128)(2,1)} %broadcast_in_dim.35), calls=%async_computation.1 | async-start | bytes 2097152 | tf_op jit(solution)/shard_map/all_to_all | solution.py:91
  125.0 206.1 %all-gather.11.cloned.1.call-start = ((), (), s32[]{:S(2)}) async-start(), calls=%async_computation.6 | async-start | bytes 10027008 | tf_op jit(solution)/shard_map/all_gather | solution.py:261
  337.7 17.4 %copy-start.14 = (f32[192,4]{0,1:T(4,128)S(1)}, f32[192,4]{0,1:T(4,128)}, u32[]{:S(2)}) copy-start(f32[192,4]{0,1:T(4,128)} %param.32) | copy-start | bytes 9220
  342.8 32.2 %all-to-all-start.5 = ((bf16[16,2,1,36,128]{4,1,3,2,0:T(2,128)(2,1)}), bf16[16,2,1,36,128]{4,1,3,2,0:T(2,128)(2,1)S(1)}, u32[]{:S(2)}, u32[]{:S(2)}) async-start(bf16[16,2,1,36,128]{4,1,3,2,0:T(2,128)(2,1)} %copy.67), calls=%async_computation.5 | async-start | bytes 589824 | tf_op jit(solution)/shard_map/all_to_all | solution.py:109
  (19 other events, 39.0 us)
Sparse Core Ops, SparseCore 0:
  242.7 88.3 all-gather.10
